TPU v7x, 32 devices: a whole 2x2x4 slice. The times are simulated.
32 devices in a mesh: ep: 8 (over z, x), tp: 4 (over y, core).
Axes of the slice: x: 2, y: 2, z: 4, core: 2. Of those that a mesh axis runs over, the one named last changes fastest.
Arguments:
- tokens: bfloat16 [192, 4096], P('ep'), may hold values from -6 to 6
- delta_state: float32 [192, 16, 128, 128], P('ep', 'tp'), may hold values from -0.625 to 0.625
- attn_gain: float32 [4096], replicated, may hold values from 0.1 to 1.9
- query_weight: bfloat16 [4096, 2048], P('ep', 'tp'), may hold values from -0.09375 to 0.09375
- key_weight: bfloat16 [4096, 2048], P('ep', 'tp'), may hold values from -0.09375 to 0.09375
- value_weight: bfloat16 [4096, 2048], P('ep', 'tp'), may hold values from -0.09375 to 0.09375
- decay_weight: bfloat16 [4096, 16], replicated, may hold values from -0.09375 to 0.09375
- beta_weight: bfloat16 [4096, 16], replicated, may hold values from -0.09375 to 0.09375
- decay_rate: float32 [16], P('tp'), may hold values from 0.05 to 3
- head_gain: float32 [128], replicated, may hold values from 0.1 to 1.9
- output_weight: bfloat16 [2048, 4096], P('tp'), may hold values from -0.125 to 0.125
- ffn_gain: float32 [4096], replicated, may hold values from 0.1 to 1.9
- expert_ids: int32 [192, 2], P('ep'), may hold values from 0 to 7, all different within a row; in each aligned block of 24 rows (0 to 23, 24 to 47, ...) at most 12 rows name the same one
- group_prob: float32 [192], P('ep'), may hold values from 0.3 to 1
- expert_logit: float32 [192, 2], P('ep'), may hold values from -8 to 8
- expert_gate: bfloat16 [8, 4096, 1024], P('ep', None, 'tp'), may hold values from -0.09375 to 0.09375
- expert_up: bfloat16 [8, 4096, 1024], P('ep', None, 'tp'), may hold values from -0.09375 to 0.09375
- expert_down: bfloat16 [8, 1024, 4096], P('ep', 'tp'), may hold values from -0.1875 to 0.1875
- dense_gate: bfloat16 [4096, 4096], P('tp', 'ep'), may hold values from -0.09375 to 0.09375
- dense_up: bfloat16 [4096, 4096], P('tp', 'ep'), may hold values from -0.09375 to 0.09375
- dense_down: bfloat16 [4096, 4096], P('ep', 'tp'), may hold values from -0.09375 to 0.09375
- dense_mix: float32 [4096], P('tp'), may hold values from -3 to 3
Outputs:
- mixed_out: bfloat16 [192, 4096], P('ep', 'tp')
- new_state: float32 [192, 16, 128, 128], P('ep', 'tp')
Inputs may be any that keep to these rules, and one draw needn't show every extreme that they name: `expert_ids`: each row names 2 different experts. Among the rows of one device (aligned blocks of 24 rows) no expert is named by more than 12 rows, and in every draw some expert reaches 12 in some block.
All inputs are finite; a program needn't handle non-finite values.
Results may differ from a plain program's by a relative error of at most 0.02.
Values may be sent and summed in bfloat16 or wider, within the bound.
A program may use at most 64 MiB of HBM per device.

v0:
```python
import jax
import jax.numpy as jnp
from jax import lax
from jax.sharding import PartitionSpec as P

EPS = 1e-06


def rms_scale(values, gain):
    mean_sq = jnp.mean(values * values, axis=-1, keepdims=True)
    return values * lax.rsqrt(mean_sq + EPS) * gain


def unit_rows(values):
    return values * lax.rsqrt(jnp.sum(values * values, axis=-1, keepdims=True) + EPS)


def per_device(
    tokens,
    delta_state,
    attn_gain,
    query_weight,
    key_weight,
    value_weight,
    decay_weight,
    beta_weight,
    decay_rate,
    head_gain,
    output_weight,
    ffn_gain,
    expert_ids,
    group_prob,
    expert_logit,
    expert_gate,
    expert_up,
    expert_down,
    dense_gate,
    dense_up,
    dense_down,
    dense_mix,
):
    seq_rows = tokens.shape[0]
    head_count = delta_state.shape[1]
    head_size = delta_state.shape[2]
    width_local = head_count * head_size
    tp_index = lax.axis_index("tp")
    residual = tokens.astype(jnp.float32)
    normed = rms_scale(residual, attn_gain).astype(jnp.bfloat16)
    spread = lax.all_to_all(normed, "ep", split_axis=1, concat_axis=0, tiled=True)
    joined = jnp.concatenate((query_weight, key_weight, value_weight), axis=1)
    summed = lax.psum_scatter(
        jnp.dot(spread, joined, preferred_element_type=jnp.float32).astype(jnp.bfloat16),
        "ep",
        scatter_dimension=0,
        tiled=True,
    ).astype(jnp.float32)
    query_sum = summed[:, :width_local]
    key_sum = summed[:, width_local : 2 * width_local]
    value_sum = summed[:, 2 * width_local :]

    def heads_of(values):
        rounded = lax.optimization_barrier(values.astype(jnp.bfloat16))
        return rounded.astype(jnp.float32).reshape(seq_rows, head_count, head_size)

    query_unit = unit_rows(heads_of(query_sum)) * head_size ** (-0.5)
    key_unit = unit_rows(heads_of(key_sum))
    value_heads = heads_of(value_sum)
    decay_cols = lax.dynamic_slice_in_dim(decay_weight, tp_index * head_count, head_count, 1)
    beta_cols = lax.dynamic_slice_in_dim(beta_weight, tp_index * head_count, head_count, 1)
    decay_pre = jnp.dot(normed, decay_cols, preferred_element_type=jnp.float32)
    decay = jnp.exp(-decay_rate * jax.nn.softplus(decay_pre))
    beta_gate = jax.nn.sigmoid(jnp.dot(normed, beta_cols, preferred_element_type=jnp.float32))
    recalled = jnp.einsum("bhk,bhkv->bhv", key_unit, delta_state, precision=lax.Precision.HIGHEST)
    correction = beta_gate[..., None] * (value_heads - decay[..., None] * recalled)
    new_state = (
        decay[..., None, None] * delta_state + key_unit[..., :, None] * correction[..., None, :]
    )
    read_out = jnp.einsum("bhk,bhkv->bhv", query_unit, new_state, precision=lax.Precision.HIGHEST)
    head_out = rms_scale(read_out, head_gain).astype(jnp.bfloat16).reshape(seq_rows, width_local)
    attn_part = jnp.dot(head_out, output_weight, preferred_element_type=jnp.float32)
    attn_sum = lax.psum(attn_part.astype(jnp.bfloat16), "tp").astype(jnp.float32)
    middle = residual + attn_sum
    ffn_in = rms_scale(middle, ffn_gain).astype(jnp.bfloat16)
    slice_width = dense_gate.shape[0]
    hidden_width = dense_gate.shape[1]
    own_columns = lax.dynamic_slice_in_dim(ffn_in, tp_index * slice_width, slice_width, 1)
    gate_up = jnp.concatenate((dense_gate, dense_up), axis=1)
    dense_part = jnp.dot(
        lax.all_gather(own_columns, "ep", axis=0, tiled=True),
        gate_up,
        preferred_element_type=jnp.float32,
    )
    dense_sum = lax.psum(dense_part.astype(jnp.bfloat16), "tp").astype(jnp.float32)
    dense_hidden = (jax.nn.silu(dense_sum[:, :hidden_width]) * dense_sum[:, hidden_width:]).astype(
        jnp.bfloat16
    )
    dense_out = lax.psum_scatter(
        jnp.dot(dense_hidden, dense_down, preferred_element_type=jnp.float32).astype(jnp.bfloat16),
        "ep",
        scatter_dimension=0,
        tiled=True,
    ).astype(jnp.float32)
    expert_count = lax.axis_size("ep")
    top_count = expert_ids.shape[1]
    capacity = max(2, 2 * seq_rows * top_count // expert_count)
    pair_ids = expert_ids.reshape(-1)
    onehot = (pair_ids[:, None] == jnp.arange(expert_count, dtype=jnp.int32)[None, :]).astype(
        jnp.int32
    )
    ranks = jnp.sum(onehot * (jnp.cumsum(onehot, axis=0) - 1), axis=1)
    places = pair_ids * capacity + ranks
    dispatch = (
        jnp.arange(expert_count * capacity, dtype=jnp.int32)[:, None] == places[None, :]
    ).astype(jnp.bfloat16)
    repeated = jnp.repeat(ffn_in, top_count, axis=0)
    outgoing = jnp.dot(dispatch, repeated, preferred_element_type=jnp.float32).astype(jnp.bfloat16)
    outgoing = outgoing.reshape(expert_count, capacity, ffn_in.shape[1])
    arrived = lax.all_to_all(outgoing, "ep", split_axis=0, concat_axis=0, tiled=True)
    gate_vals = jnp.einsum(
        "snd,df->snf", arrived, expert_gate[0], preferred_element_type=jnp.float32
    )
    up_vals = jnp.einsum("snd,df->snf", arrived, expert_up[0], preferred_element_type=jnp.float32)
    expert_hidden = (jax.nn.silu(gate_vals) * up_vals).astype(jnp.bfloat16)
    partial_value = jnp.einsum(
        "snf,fd->snd", expert_hidden, expert_down[0], preferred_element_type=jnp.float32
    )
    summed_cols = lax.psum_scatter(
        partial_value.astype(jnp.bfloat16), "tp", scatter_dimension=2, tiled=True
    )
    returned = lax.all_to_all(summed_cols, "ep", split_axis=0, concat_axis=0, tiled=True)
    flat_back = returned.reshape(expert_count * capacity, slice_width)
    picked = (
        jnp.take(flat_back, places, axis=0)
        .astype(jnp.float32)
        .reshape(seq_rows, top_count, slice_width)
    )
    logit_exp = jnp.exp(expert_logit)
    route_weight = group_prob[:, None] * logit_exp / jnp.sum(logit_exp, axis=1, keepdims=True)
    expert_mix = jnp.sum(route_weight[..., None] * picked, axis=1)
    own_middle = lax.dynamic_slice_in_dim(middle, tp_index * slice_width, slice_width, 1)
    mixed_out = (own_middle + jax.nn.sigmoid(dense_mix) * dense_out + expert_mix).astype(
        jnp.bfloat16
    )
    return (mixed_out, new_state)


def solution(mesh):
    return jax.shard_map(
        per_device,
        mesh=mesh,
        in_specs=(
            P("ep", None),
            P("ep", "tp", None, None),
            P(),
            P("ep", "tp"),
            P("ep", "tp"),
            P("ep", "tp"),
            P(),
            P(),
            P("tp"),
            P(),
            P("tp", None),
            P(),
            P("ep", None),
            P("ep"),
            P("ep", None),
            P("ep", None, "tp"),
            P("ep", None, "tp"),
            P("ep", "tp", None),
            P("tp", "ep"),
            P("tp", "ep"),
            P("ep", "tp"),
            P("tp"),
        ),
        out_specs=(P("ep", "tp"), P("ep", "tp", None, None)),
        check_vma=False,
    )
```

profile of v0, /device:TPU:0, one launch (start us, length us, event | category | flops | bytes accessed | tf_op | source)
XLA Modules:
  0.0 333.8 jit_solution(11705922929324244987)
XLA Ops:
  7.2 1.2 fusion.28
  8.4 1.1 fusion.30
  9.6 15.0 %all_to_all.29 = bf16[24,8,512]{2,0,1:T(8,128)(2,1)S(1)} all-to-all(bf16[24,8,512]{2,0,1:T(8,128)(2,1)S(1)} %bitcast.59), channel_id=1, replica_groups=mesh['ep'=8,'tp'=4] {'ep'}, dimensions={1} | all-to-all | bytes 393216 | tf_op jit(solution)/shard_map/all_to_all | solution.py:49
  24.6 2.7 convolution_convert_fusion.3
  27.4 1.0 fusion.48
  28.4 0.1 copy.67
  28.5 1.0 fusion.27
  29.5 0.1 copy.68
  29.6 0.1 copy.73
  29.7 0.1 reshape.151
  30.0 0.2 select_reduce_fusion
  30.1 58.6 %reduce-scatter.4.cloned.1.call-done = bf16[24,1536]{1,0:T(8,128)(2,1)} async-done(((bf16[192,1536]{1,0:T(8,128)(2,1)}), bf16[24,1536]{1,0:T(8,128)(2,1)}) %reduce-scatter.4.cloned.1.call-update) | async-done | bytes 73744 | tf_op jit(solution)/shard_map/reduce_scatter | solution.py:51
  88.8 0.8 fusion.58
  89.6 0.1 multiply_reduce_fusion.3
  89.7 0.1 broadcast_multiply_fusion
  89.8 8.1 %fusion.59 = f32[24,4,1,128]{3,2,1,0:T(1,128)S(1)} fusion(f32[24,4,128,1]{2,3,1,0:T(1,128)S(1)} %bitcast.60, f32[24,4,128,128]{3,2,1,0:T(8,128)} %param.23), kind=kOutput, calls=%fused_computation.93 | convolution fusion | flops 18874368 | bytes 6389760 | tf_op jit(solution)/shard_map/bhk,bhkv->bhv/dot_general | solution.py:73
  97.9 0.1 subtract_multiply_fusion
  98.1 3.9 %multiply_add_fusion = f32[24,4,128,128]{3,2,1,0:T(8,128)} fusion(f32[24,4,128,128]{3,2,1,0:T(8,128)S(1)} %copy-done.1, f32[24,4,128]{2,1,0:T(4,128)S(1)} %subtract_multiply_fusion, f32[24,4,128]{2,1,0:T(4,128)S(1)} %broadcast_multiply_fusion, f32[24,4]{1,0:T(8,128)S(1)} %copy.67), kind=kLoop, calls=%fused_computation.1 | loop fusion | flops 4718592 | bytes 12681600 | tf_op jit(solution)/shard_map/add | solution.py:76
  101.9 0.1 multiply_reduce_fusion.4
  102.1 0.1 multiply_multiply_fusion
  102.2 7.5 %fusion.60 = f32[24,4,1,128]{3,2,1,0:T(1,128)S(1)} fusion(f32[24,4,128,1]{2,3,1,0:T(1,128)S(1)} %bitcast.63, f32[24,4,128,128]{3,2,1,0:T(8,128)} %multiply_add_fusion), kind=kOutput, calls=%fused_computation.94 | convolution fusion | flops 18874368 | bytes 6389760 | tf_op jit(solution)/shard_map/bhk,bhkv->bhv/dot_general | solution.py:78
  109.7 0.1 multiply_reduce_fusion.2
  109.8 0.1 multiply_convert_fusion.1
  109.9 1.4 convolution_convert_fusion.2
  111.3 31.2 %all-reduce.3.cloned.1.call-done = bf16[24,4096]{1,0:T(8,128)(2,1)} async-done(((bf16[24,4096]{1,0:T(8,128)(2,1)}), bf16[24,4096]{1,0:T(8,128)(2,1)}) %all-reduce.3.cloned.1.call-update) | async-done | bytes 196624 | tf_op jit(solution)/shard_map/psum | solution.py:81
  142.5 1.8 convert_add_fusion
  144.3 1.0 multiply_convert_fusion
  145.4 0.3 broadcast_in_dim.10
  145.7 0.2 reshape.152
  145.9 0.3 convolution_convert_fusion.1
  146.2 1.2 reshape.153
  147.4 5.5 %all-to-all-start.1 = ((bf16[8,12,4096]{2,1,0:T(8,128)(2,1)}), bf16[8,12,4096]{2,1,0:T(8,128)(2,1)S(1)}, u32[]{:S(2)}, u32[]{:S(2)}) async-start(bf16[8,12,4096]{2,1,0:T(8,128)(2,1)} %reshape.153), calls=%async_computation.3 | async-start | bytes 2097152 | tf_op jit(solution)/shard_map/all_to_all | solution.py:118
  153.0 45.7 %all_gather.3 = bf16[192,1024]{1,0:T(8,128)(2,1)S(1)} all-gather(bf16[24,1024]{1,0:T(8,128)(2,1)S(1)} %constant_dynamic-slice_fusion), channel_id=1, replica_groups=mesh['ep'=8,'tp'=4] {'ep'}, dimensions={0}, use_global_device_ids=true | all-gather | bytes 442368 | tf_op jit(solution)/shard_map/all_gather | solution.py:89
  198.6 2.9 fusion.14
  201.6 2.0 fusion.7
  203.7 3.9 %convolution_convert_fusion = bf16[8,12,4096]{2,1,0:T(8,128)(2,1)} fusion(bf16[1,256,4096]{2,1,0:T(8,128)(2,1)S(1)} %copy-done, bf16[8,12,4096]{2,1,0:T(8,128)(2,1)S(1)} %all-to-all-done.1, bf16[1,4096,256]{2,1,0:T(8,128)(2,1)} %param.38, f32[8,12,256]{2,1,0:T(8,128)S(1)} %fusion.7), kind=kOutput, calls=%fused_computation.2 | convolution fusion | flops 403193856 | bytes 5865472 | tf_op jit(solution)/shard_map/snf,fd->snd/dot_general | solution.py:124
  207.9 25.3 %all-reduce.5.cloned.1.call-done = bf16[192,1024]{1,0:T(8,128)(2,1)} async-done(((bf16[192,1024]{1,0:T(8,128)(2,1)}), bf16[192,1024]{1,0:T(8,128)(2,1)}) %all-reduce.5.cloned.1.call-update) | async-done | bytes 393232 | tf_op jit(solution)/shard_map/psum | solution.py:93
  233.2 1.1 convert_element_type.71
  234.3 2.4 convolution_convert_fusion.4
  236.8 0.1 mul.260
  236.9 23.5 %reduce-scatter.8.cloned.1.call-done = bf16[8,12,1024]{2,1,0:T(8,128)(2,1)} async-done(((bf16[8,12,4096]{2,1,0:T(8,128)(2,1)}), bf16[8,12,1024]{2,1,0:T(8,128)(2,1)}) %reduce-scatter.8.cloned.1.call-update) | async-done | bytes 196624 | tf_op jit(solution)/shard_map/reduce_scatter | solution.py:127
  260.4 5.5 %all-to-all-start.2 = ((bf16[8,12,1024]{2,1,0:T(8,128)(2,1)}), bf16[8,12,1024]{2,1,0:T(8,128)(2,1)S(1)}, u32[]{:S(2)}, u32[]{:S(2)}) async-start(bf16[8,12,1024]{2,1,0:T(8,128)(2,1)} %reduce-scatter.8.cloned.1.call-done), calls=%async_computation.5 | async-start | bytes 524288 | tf_op jit(solution)/shard_map/all_to_all | solution.py:130
  265.9 0.1 copy.75
  266.1 9.1 %all-to-all-done.2 = bf16[8,12,1024]{2,1,0:T(8,128)(2,1)S(1)} async-done(((bf16[8,12,1024]{2,1,0:T(8,128)(2,1)}), bf16[8,12,1024]{2,1,0:T(8,128)(2,1)S(1)}, u32[]{:S(2)}, u32[]{:S(2)}) %all-to-all-start.2) | async-done | bytes 196640 | tf_op jit(solution)/shard_map/all_to_all | solution.py:130
  275.2 0.7 gather_fusion
  276.0 0.4 multiply_reduce_fusion.1
  276.4 49.3 %reduce-scatter.6.cloned.1.call-done = bf16[24,1024]{1,0:T(8,128)(2,1)} async-done(((bf16[192,1024]{1,0:T(8,128)(2,1)}), bf16[24,1024]{1,0:T(8,128)(2,1)}) %reduce-scatter.6.cloned.1.call-update) | async-done | bytes 49168 | tf_op jit(solution)/shard_map/reduce_scatter | solution.py:97
  325.7 1.6 add_convert_fusion
  (60 shorter events, 1.1 us)
Async XLA Ops:
  7.2 196.5 %copy-start = (bf16[1,256,4096]{2,1,0:T(8,128)(2,1)S(1)}, bf16[1,256,4096]{2,1,0:T(8,128)(2,1)}, u32[]{:S(2)}) copy-start(bf16[1,256,4096]{2,1,0:T(8,128)(2,1)} %param.39) | copy-start | bytes 6291460
  7.2 81.6 %reduce-scatter.4.cloned.1.call-start = ((), (), s32[]{:S(2)}) async-start(), calls=%async_computation.6 | async-start | bytes 663552 | tf_op jit(solution)/shard_map/reduce_scatter | solution.py:51
  9.5 17.8 %copy-start.10 = (f32[4]{0:T(128)S(1)}, f32[4]{0:T(128)}, u32[]{:S(2)}) copy-start(f32[4]{0:T(128)} %param.30) | copy-start | bytes 52
  9.5 20.1 %copy-start.5 = (s32[24,2]{0,1:T(2,128)S(1)}, s32[24,2]{0,1:T(2,128)}, u32[]{:S(2)}) copy-start(s32[24,2]{0,1:T(2,128)} %param.34) | copy-start | bytes 580
  27.3 115.2 %all-reduce.3.cloned.1.call-start = ((), (), s32[]{:S(2)}) async-start(), calls=%async_computation.7 | async-start | bytes 393216 | tf_op jit(solution)/shard_map/psum | solution.py:81
  89.8 8.2 %copy-start.1 = (f32[24,4,128,128]{3,2,1,0:T(8,128)S(1)}, f32[24,4,128,128]{3,2,1,0:T(8,128)}, u32[]{:S(2)}) copy-start(f32[24,4,128,128]{3,2,1,0:T(8,128)} %param.23) | copy-start | bytes 18874372
  102.2 7.6 %copy-start.8 = (f32[128]{0:T(128)S(1)}, f32[128]{0:T(128)}, u32[]{:S(2)}) copy-start(f32[128]{0:T(128)} %param.31) | copy-start | bytes 1540
  102.2 7.7 %copy-start.2 = (bf16[512,4096]{1,0:T(8,128)(2,1)S(1)}, bf16[512,4096]{1,0:T(8,128)(2,1)}, u32[]{:S(2)}) copy-start(bf16[512,4096]{1,0:T(8,128)(2,1)} %param.32) | copy-start | bytes 12582916
  109.7 32.8 %copy-start.3 = (bf16[24,4096]{1,0:T(8,128)(2,1)S(1)}, bf16[24,4096]{1,0:T(8,128)(2,1)}, u32[]{:S(2)}) copy-start(bf16[24,4096]{1,0:T(8,128)(2,1)} %param.22) | copy-start | bytes 589828
  109.7 34.7 %copy-start.4 = (f32[4096]{0:T(1024)S(1)}, f32[4096]{0:T(1024)}, u32[]{:S(2)}) copy-start(f32[4096]{0:T(1024)} %param.33) | copy-start | bytes 49156
  147.4 54.2 %all-to-all-start.1 = ((bf16[8,12,4096]{2,1,0:T(8,128)(2,1)}), bf16[8,12,4096]{2,1,0:T(8,128)(2,1)S(1)}, u32[]{:S(2)}, u32[]{:S(2)}) async-start(bf16[8,12,4096]{2,1,0:T(8,128)(2,1)} %reshape.153), calls=%async_computation.3 | async-start | bytes 2097152 | tf_op jit(solution)/shard_map/all_to_all | solution.py:118
  152.9 80.3 %all-reduce.5.cloned.1.call-start = ((), (), s32[]{:S(2)}) async-start(), calls=%async_computation.8 | async-start | bytes 786432 | tf_op jit(solution)/shard_map/psum | solution.py:93
  201.5 58.9 %reduce-scatter.8.cloned.1.call-start = ((), (), s32[]{:S(2)}) async-start(), calls=%async_computation.10 | async-start | bytes 1310720 | tf_op jit(solution)/shard_map/reduce_scatter | solution.py:127
  203.7 4.2 %copy-start.7 = (f32[24,2]{0,1:T(2,128)S(1)}, f32[24,2]{0,1:T(2,128)}, u32[]{:S(2)}) copy-start(f32[24,2]{0,1:T(2,128)} %param.36) | copy-start | bytes 580
  203.7 4.2 %copy-start.9 = (f32[24]{0:T(128)S(1)}, f32[24]{0:T(128)}, u32[]{:S(2)}) copy-start(f32[24]{0:T(128)} %param.35) | copy-start | bytes 292
  207.6 58.5 %copy-start.6 = (f32[1024]{0:T(1024)S(1)}, f32[1024]{0:T(1024)}, u32[]{:S(2)}) copy-start(f32[1024]{0:T(1024)} %param.43) | copy-start | bytes 12292
  207.6 118.1 %reduce-scatter.6.cloned.1.call-start = ((), (), s32[]{:S(2)}) async-start(), calls=%async_computation.9 | async-start | bytes 442368 | tf_op jit(solution)/shard_map/reduce_scatter | solution.py:97
  260.4 14.8 %all-to-all-start.2 = ((bf16[8,12,1024]{2,1,0:T(8,128)(2,1)}), bf16[8,12,1024]{2,1,0:T(8,128)(2,1)S(1)}, u32[]{:S(2)}, u32[]{:S(2)}) async-start(bf16[8,12,1024]{2,1,0:T(8,128)(2,1)} %reduce-scatter.8.cloned.1.call-done), calls=%async_computation.5 | async-start | bytes 524288 | tf_op jit(solution)/shard_map/all_to_all | solution.py:130
Sparse Core Ops, SparseCore 0:
  27.4 61.3 reduce-scatter.3
  111.4 31.0 all-reduce.2
  201.7 31.4 all-reduce.4
  235.6 24.7 reduce-scatter.7
  263.5 62.1 reduce-scatter.5
where the time goes:
time: 335 us; the launch traced here: 334 us
  waiting for transfers between devices  197 us (59%)
  blocking collectives  60.7 us (18%)
  matrix products  33.2 us (10%)
  between operations  14.1 us (4%)
  other arithmetic  13.2 us (4%)
  starting transfers between devices  11.2 us (3%)
  local copies, waits for them, and re-layouts  4.25 us (1%)
    reduce_scatter x1, waiting for transfers between devices, per_device(): lax.psum_scatter(jnp.dot(spread, joined, preferred_element_type=jnp.float...  58.6 us
    reduce_scatter x1, waiting for transfers between devices, per_device(): lax.psum_scatter(jnp.dot(dense_hidden, dense_down, preferred_element_type...  49.3 us
    all_gather x1, blocking collectives, per_device(): lax.all_gather(own_columns, 'ep', axis=0, tiled=True)  45.7 us
    psum x1, waiting for transfers between devices, per_device(): lax.psum(attn_part.astype(jnp.bfloat16), 'tp').astype(jnp.float32)  31.2 us
    psum x1, waiting for transfers between devices, per_device(): lax.psum(dense_part.astype(jnp.bfloat16), 'tp').astype(jnp.float32)  25.3 us
    reduce_scatter x1, waiting for transfers between devices, per_device(): lax.psum_scatter(partial_value.astype(jnp.bfloat16), 'tp', scatter_dimens...  23.5 us
    all_to_all x1, blocking collectives, per_device(): lax.all_to_all(normed, 'ep', split_axis=1, concat_axis=0, tiled=True)  15 us
    all_to_all x1, waiting for transfers between devices, per_device(): lax.all_to_all(summed_cols, 'ep', split_axis=0, concat_axis=0, tiled=True)  9.06 us
  transfers between devices with their start and end apart: 7, of which 6 were waited for; matrix products, arithmetic and copies ran while one was open for 5% of the time, Pallas kernels for 0%

commit v1 on v0

--- a/solution.py
+++ b/solution.py
@@ -4,6 +4,11 @@
 from jax.sharding import PartitionSpec as P
 
 EPS = 1e-06
+
+
+def summed_here(block, axis):
+    terms = lax.all_gather(block, axis)
+    return jnp.sum(terms, axis=0)
 
 
 def rms_scale(values, gain):
@@ -90,7 +95,7 @@
         gate_up,
         preferred_element_type=jnp.float32,
     )
-    dense_sum = lax.psum(dense_part.astype(jnp.bfloat16), "tp").astype(jnp.float32)
+    dense_sum = summed_here(dense_part.astype(jnp.bfloat16), "tp").astype(jnp.float32)
     dense_hidden = (jax.nn.silu(dense_sum[:, :hidden_width]) * dense_sum[:, hidden_width:]).astype(
         jnp.bfloat16
     )

time: 335 us -> 309 us (0.922)
  waiting for transfers between devices: 197 us -> 167 us
  blocking collectives: 60.7 us -> 70.3 us
  starting transfers between devices: 11.2 us -> 5.71 us
    psum x1 -> x0, waiting for transfers between devices: 25.3 us -> none  [per_device(): lax.psum(dense_part.astype(jnp.bfloat16), 'tp').astype(jnp.float32)]
    all_to_all x0 -> x1, blocking collectives: none -> 24.1 us  [per_device(): lax.all_to_all(outgoing, 'ep', split_axis=0, concat_axis=0, tiled=True)]
    all_gather x1, blocking collectives: 45.7 us -> 31.2 us  [per_device(): lax.all_gather(own_columns, 'ep', axis=0, tiled=True)]
    all_to_all x1 -> x0, starting transfers between devices: 5.51 us -> none  [per_device(): lax.all_to_all(outgoing, 'ep', split_axis=0, concat_axis=0, tiled=True)]
    reduce_scatter x1, waiting for transfers between devices: 23.5 us -> 18.8 us  [per_device(): lax.psum_scatter(partial_value.astype(jnp.bfloat16), 'tp', scatter_dimens...]
  transfers between devices with their start and end apart: 7 -> 6, of which waited for: 6 -> 5; matrix products, arithmetic and copies ran while one was open for 5% -> 5% of each run, Pallas kernels for 0% -> 0%
where the time goes in v1:
time: 309 us
  waiting for transfers between devices  167 us (54%)
  blocking collectives  70.3 us (23%)
  matrix products  33.2 us (11%)
  between operations  14.2 us (5%)
  other arithmetic  13.9 us (4%)
  starting transfers between devices  5.71 us (2%)
  local copies, waits for them, and re-layouts  4.23 us (1%)
    reduce_scatter x1, waiting for transfers between devices, per_device(): lax.psum_scatter(jnp.dot(spread, joined, preferred_element_type=jnp.float...  58.8 us
    reduce_scatter x1, waiting for transfers between devices, per_device(): lax.psum_scatter(jnp.dot(dense_hidden, dense_down, preferred_element_type...  49.4 us
    all_gather x1, blocking collectives, per_device(): lax.all_gather(own_columns, 'ep', axis=0, tiled=True)  31.2 us
    psum x1, waiting for transfers between devices, per_device(): lax.psum(attn_part.astype(jnp.bfloat16), 'tp').astype(jnp.float32)  31 us
    all_to_all x1, blocking collectives, per_device(): lax.all_to_all(outgoing, 'ep', split_axis=0, concat_axis=0, tiled=True)  24.1 us
    reduce_scatter x1, waiting for transfers between devices, per_device(): lax.psum_scatter(partial_value.astype(jnp.bfloat16), 'tp', scatter_dimens...  18.8 us
    all_to_all x1, blocking collectives, per_device(): lax.all_to_all(normed, 'ep', split_axis=1, concat_axis=0, tiled=True)  15 us
    all_to_all x1, waiting for transfers between devices, per_device(): lax.all_to_all(summed_cols, 'ep', split_axis=0, concat_axis=0, tiled=True)  9 us
  transfers between devices with their start and end apart: 6, of which 5 were waited for; matrix products, arithmetic and copies ran while one was open for 5% of the time, Pallas kernels for 0%

profile of v1, /device:TPU:0, one launch (start us, length us, event | category | flops | bytes accessed | tf_op | source)
XLA Modules:
  0.0 308.6 jit_solution(11541364711296302137)
XLA Ops:
  7.2 1.2 fusion.28
  8.4 1.1 fusion.30
  9.6 15.0 %all_to_all.29 = bf16[24,8,512]{2,0,1:T(8,128)(2,1)S(1)} all-to-all(bf16[24,8,512]{2,0,1:T(8,128)(2,1)S(1)} %bitcast.61), channel_id=1, replica_groups=mesh['ep'=8,'tp'=4] {'ep'}, dimensions={1} | all-to-all | bytes 393216 | tf_op jit(solution)/shard_map/all_to_all | solution.py:54
  24.6 2.7 convolution_convert_fusion.3
  27.4 1.0 fusion.48
  28.4 0.1 copy.67
  28.5 1.0 fusion.27
  29.5 0.1 copy.68
  29.6 0.1 copy.73
  29.7 0.1 reshape.151
  30.0 58.8 %reduce-scatter.4.cloned.1.call-done = bf16[24,1536]{1,0:T(8,128)(2,1)} async-done(((bf16[192,1536]{1,0:T(8,128)(2,1)}), bf16[24,1536]{1,0:T(8,128)(2,1)}) %reduce-scatter.4.cloned.1.call-update) | async-done | bytes 73744 | tf_op jit(solution)/shard_map/reduce_scatter | solution.py:56
  88.8 0.8 fusion.58
  89.6 0.1 multiply_reduce_fusion.3
  89.7 0.1 broadcast_multiply_fusion
  89.8 8.1 %fusion.59 = f32[24,4,1,128]{3,2,1,0:T(1,128)S(1)} fusion(f32[24,4,128,1]{2,3,1,0:T(1,128)S(1)} %bitcast.62, f32[24,4,128,128]{3,2,1,0:T(8,128)} %param.23), kind=kOutput, calls=%fused_computation.93 | convolution fusion | flops 18874368 | bytes 6389760 | tf_op jit(solution)/shard_map/bhk,bhkv->bhv/dot_general | solution.py:78
  97.9 0.1 subtract_multiply_fusion
  98.1 3.9 %multiply_add_fusion = f32[24,4,128,128]{3,2,1,0:T(8,128)} fusion(f32[24,4,128,128]{3,2,1,0:T(8,128)S(1)} %copy-done.1, f32[24,4,128]{2,1,0:T(4,128)S(1)} %subtract_multiply_fusion, f32[24,4,128]{2,1,0:T(4,128)S(1)} %broadcast_multiply_fusion, f32[24,4]{1,0:T(8,128)S(1)} %copy.67), kind=kLoop, calls=%fused_computation.1 | loop fusion | flops 4718592 | bytes 12681600 | tf_op jit(solution)/shard_map/add | solution.py:81
  101.9 0.1 multiply_reduce_fusion.4
  102.1 0.1 multiply_multiply_fusion
  102.2 7.5 %fusion.60 = f32[24,4,1,128]{3,2,1,0:T(1,128)S(1)} fusion(f32[24,4,128,1]{2,3,1,0:T(1,128)S(1)} %bitcast.65, f32[24,4,128,128]{3,2,1,0:T(8,128)} %multiply_add_fusion), kind=kOutput, calls=%fused_computation.94 | convolution fusion | flops 18874368 | bytes 6389760 | tf_op jit(solution)/shard_map/bhk,bhkv->bhv/dot_general | solution.py:83
  109.7 0.1 multiply_reduce_fusion.2
  109.8 0.1 multiply_convert_fusion.1
  109.9 1.4 convolution_convert_fusion.2
  111.3 0.2 select_reduce_fusion
  111.5 31.0 %all-reduce.2.cloned.1.call-done = bf16[24,4096]{1,0:T(8,128)(2,1)} async-done(((bf16[24,4096]{1,0:T(8,128)(2,1)}), bf16[24,4096]{1,0:T(8,128)(2,1)}) %all-reduce.2.cloned.1.call-update) | async-done | bytes 196624 | tf_op jit(solution)/shard_map/psum | solution.py:86
  142.5 1.8 convert_add_fusion
  144.3 1.0 multiply_convert_fusion
  145.4 31.2 %all_gather.9 = bf16[192,1024]{1,0:T(8,128)(2,1)S(1)} all-gather(bf16[24,1024]{1,0:T(8,128)(2,1)S(1)} %constant_dynamic-slice_fusion), channel_id=1, replica_groups=mesh['ep'=8,'tp'=4] {'ep'}, dimensions={0}, use_global_device_ids=true | all-gather | bytes 442368 | tf_op jit(solution)/shard_map/all_gather | solution.py:94
  176.6 2.9 fusion.14
  179.6 0.3 broadcast_in_dim.10
  179.9 0.2 reshape.152
  180.1 0.3 convolution_convert_fusion.1
  180.4 1.1 reshape.153
  181.6 24.1 %all_to_all.30 = bf16[8,12,4096]{2,1,0:T(8,128)(2,1)S(1)} all-to-all(bf16[8,12,4096]{2,1,0:T(8,128)(2,1)} %reshape.153), channel_id=1, replica_groups=mesh['ep'=8,'tp'=4] {'ep'}, dimensions={0} | all-to-all | bytes 1572864 | tf_op jit(solution)/shard_map/all_to_all | solution.py:123
  205.6 2.0 fusion.7
  207.7 3.9 %convolution_convert_fusion = bf16[8,12,4096]{2,1,0:T(8,128)(2,1)} fusion(bf16[1,256,4096]{2,1,0:T(8,128)(2,1)S(1)} %copy-done, bf16[8,12,4096]{2,1,0:T(8,128)(2,1)S(1)} %all_to_all.30, bf16[1,4096,256]{2,1,0:T(8,128)(2,1)} %param.38, f32[8,12,256]{2,1,0:T(8,128)S(1)} %fusion.7), kind=kOutput, calls=%fused_computation.2 | convolution fusion | flops 403193856 | bytes 5865472 | tf_op jit(solution)/shard_map/snf,fd->snd/dot_general | solution.py:129
  212.0 1.7 reduce_sum.93
  213.8 2.4 convolution_convert_fusion.4
  216.2 0.1 copy.76
  216.3 0.1 mul.260
  216.4 18.8 %reduce-scatter.8.cloned.1.call-done = bf16[8,12,1024]{2,1,0:T(8,128)(2,1)} async-done(((bf16[8,12,4096]{2,1,0:T(8,128)(2,1)}), bf16[8,12,1024]{2,1,0:T(8,128)(2,1)}) %reduce-scatter.8.cloned.1.call-update) | async-done | bytes 196624 | tf_op jit(solution)/shard_map/reduce_scatter | solution.py:132
  235.2 5.5 %all-to-all-start.2 = ((bf16[8,12,1024]{2,1,0:T(8,128)(2,1)}), bf16[8,12,1024]{2,1,0:T(8,128)(2,1)S(1)}, u32[]{:S(2)}, u32[]{:S(2)}) async-start(bf16[8,12,1024]{2,1,0:T(8,128)(2,1)} %reduce-scatter.8.cloned.1.call-done), calls=%async_computation.5 | async-start | bytes 524288 | tf_op jit(solution)/shard_map/all_to_all | solution.py:135
  240.7 0.1 copy.75
  240.9 9.0 %all-to-all-done.2 = bf16[8,12,1024]{2,1,0:T(8,128)(2,1)S(1)} async-done(((bf16[8,12,1024]{2,1,0:T(8,128)(2,1)}), bf16[8,12,1024]{2,1,0:T(8,128)(2,1)S(1)}, u32[]{:S(2)}, u32[]{:S(2)}) %all-to-all-start.2) | async-done | bytes 196640 | tf_op jit(solution)/shard_map/all_to_all | solution.py:135
  250.0 0.7 gather_fusion
  250.7 0.4 multiply_reduce_fusion.1
  251.1 49.4 %reduce-scatter.6.cloned.1.call-done = bf16[24,1024]{1,0:T(8,128)(2,1)} async-done(((bf16[192,1024]{1,0:T(8,128)(2,1)}), bf16[24,1024]{1,0:T(8,128)(2,1)}) %reduce-scatter.6.cloned.1.call-update) | async-done | bytes 49168 | tf_op jit(solution)/shard_map/reduce_scatter | solution.py:102
  300.5 1.6 add_convert_fusion
  (60 shorter events, 1.1 us)
Async XLA Ops:
  7.2 200.5 %copy-start = (bf16[1,256,4096]{2,1,0:T(8,128)(2,1)S(1)}, bf16[1,256,4096]{2,1,0:T(8,128)(2,1)}, u32[]{:S(2)}) copy-start(bf16[1,256,4096]{2,1,0:T(8,128)(2,1)} %param.39) | copy-start | bytes 6291460
  7.2 81.6 %reduce-scatter.4.cloned.1.call-start = ((), (), s32[]{:S(2)}) async-start(), calls=%async_computation.6 | async-start | bytes 663552 | tf_op jit(solution)/shard_map/reduce_scatter | solution.py:56
  9.5 17.8 %copy-start.10 = (f32[4]{0:T(128)S(1)}, f32[4]{0:T(128)}, u32[]{:S(2)}) copy-start(f32[4]{0:T(128)} %param.30) | copy-start | bytes 52
  9.5 20.1 %copy-start.5 = (s32[24,2]{0,1:T(2,128)S(1)}, s32[24,2]{0,1:T(2,128)}, u32[]{:S(2)}) copy-start(s32[24,2]{0,1:T(2,128)} %param.34) | copy-start | bytes 580
  27.3 115.2 %all-reduce.2.cloned.1.call-start = ((), (), s32[]{:S(2)}) async-start(), calls=%async_computation.7 | async-start | bytes 393216 | tf_op jit(solution)/shard_map/psum | solution.py:86
  89.8 8.2 %copy-start.1 = (f32[24,4,128,128]{3,2,1,0:T(8,128)S(1)}, f32[24,4,128,128]{3,2,1,0:T(8,128)}, u32[]{:S(2)}) copy-start(f32[24,4,128,128]{3,2,1,0:T(8,128)} %param.23) | copy-start | bytes 18874372
  102.2 7.6 %copy-start.8 = (f32[128]{0:T(128)S(1)}, f32[128]{0:T(128)}, u32[]{:S(2)}) copy-start(f32[128]{0:T(128)} %param.31) | copy-start | bytes 1540
  102.2 7.7 %copy-start.2 = (bf16[512,4096]{1,0:T(8,128)(2,1)S(1)}, bf16[512,4096]{1,0:T(8,128)(2,1)}, u32[]{:S(2)}) copy-start(bf16[512,4096]{1,0:T(8,128)(2,1)} %param.32) | copy-start | bytes 12582916
  109.7 32.8 %copy-start.3 = (bf16[24,4096]{1,0:T(8,128)(2,1)S(1)}, bf16[24,4096]{1,0:T(8,128)(2,1)}, u32[]{:S(2)}) copy-start(bf16[24,4096]{1,0:T(8,128)(2,1)} %param.22) | copy-start | bytes 589828
  109.7 34.7 %copy-start.4 = (f32[4096]{0:T(1024)S(1)}, f32[4096]{0:T(1024)}, u32[]{:S(2)}) copy-start(f32[4096]{0:T(1024)} %param.33) | copy-start | bytes 49156
  111.3 100.7 %all-gather.3.cloned.1.call-start = ((), (), s32[]{:S(2)}) async-start(), calls=%async_computation.10 | async-start | bytes 1966080 | tf_op jit(solution)/shard_map/all_gather | solution.py:10
  179.5 55.7 %reduce-scatter.8.cloned.1.call-start = ((), (), s32[]{:S(2)}) async-start(), calls=%async_computation.9 | async-start | bytes 1310720 | tf_op jit(solution)/shard_map/reduce_scatter | solution.py:132
  207.7 4.2 %copy-start.7 = (f32[24,2]{0,1:T(2,128)S(1)}, f32[24,2]{0,1:T(2,128)}, u32[]{:S(2)}) copy-start(f32[24,2]{0,1:T(2,128)} %param.36) | copy-start | bytes 580
  207.7 4.2 %copy-start.9 = (f32[24]{0:T(128)S(1)}, f32[24]{0:T(128)}, u32[]{:S(2)}) copy-start(f32[24]{0:T(128)} %param.35) | copy-start | bytes 292
  211.6 88.8 %reduce-scatter.6.cloned.1.call-start = ((), (), s32[]{:S(2)}) async-start(), calls=%async_computation.8 | async-start | bytes 442368 | tf_op jit(solution)/shard_map/reduce_scatter | solution.py:102
  211.9 29.0 %copy-start.6 = (f32[1024]{0:T(1024)S(1)}, f32[1024]{0:T(1024)}, u32[]{:S(2)}) copy-start(f32[1024]{0:T(1024)} %param.43) | copy-start | bytes 12292
  235.2 14.7 %all-to-all-start.2 = ((bf16[8,12,1024]{2,1,0:T(8,128)(2,1)}), bf16[8,12,1024]{2,1,0:T(8,128)(2,1)S(1)}, u32[]{:S(2)}, u32[]{:S(2)}) async-start(bf16[8,12,1024]{2,1,0:T(8,128)(2,1)} %reduce-scatter.8.cloned.1.call-done), calls=%async_computation.5 | async-start | bytes 524288 | tf_op jit(solution)/shard_map/all_to_all | solution.py:135
Sparse Core Ops, SparseCore 0:
  27.4 61.3 reduce-scatter.3
  111.4 31.0 all-reduce.1
  179.7 19.3 all-gather.2
  211.7 23.4 reduce-scatter.7
  238.3 62.1 reduce-scatter.5
